TPU v7x, 32 devices: a whole 2x2x4 slice. The times are simulated.
32 devices in a mesh: fs: 8 (over z, y), tp: 4 (over x, core).
Axes of the slice: x: 2, y: 2, z: 4, core: 2. Of those that a mesh axis runs over, the one named last changes fastest.
Arguments:
- x_late: bfloat16 [6144, 2048], P(('fs', 'tp')), may hold values from -6 to 6
- x_early: bfloat16 [6144, 2048], P(('fs', 'tp')), may hold values from -6 to 6
- w_gate: bfloat16 [2048, 5632], P('fs', 'tp'), may hold values from -0.125 to 0.125
- w_value: bfloat16 [2048, 5632], P('fs', 'tp'), may hold values from -0.125 to 0.125
- conv_taps: float32 [3, 5632], P(None, 'tp'), may hold values from -3 to 3
- grad_hidden: bfloat16 [6144, 5632], P('fs', 'tp'), may hold values from -6 to 6
- sum_gate: float32 [2048, 5632], P('fs', 'tp'), may hold values from -6 to 6
- sum_value: float32 [2048, 5632], P('fs', 'tp'), may hold values from -6 to 6
- sum_taps: float32 [3, 5632], P(None, 'tp'), may hold values from -6 to 6
Outputs:
- hidden_late: bfloat16 [6144, 5632], P('fs', 'tp')
- grad_early: bfloat16 [6144, 2048], P(('fs', 'tp'))
- new_sum_gate: float32 [2048, 5632], P('fs', 'tp')
- new_sum_value: float32 [2048, 5632], P('fs', 'tp')
- new_sum_taps: float32 [3, 5632], P(None, 'tp')
All inputs are finite; a program needn't handle non-finite values.
Results may differ from a plain program's by a relative error of at most 0.015.
Values may be sent and summed in bfloat16 or wider, within the bound.
A program may use at most 128 MiB of HBM per device.

v0:
```python
import math
import jax
import jax.numpy as jnp
from jax import lax
from jax.sharding import PartitionSpec as P

root_half = 0.7071067811865476
density_norm = 0.3989422804014327


def causal_mix(gate_rows, taps):
    width = taps.shape[0]
    length = gate_rows.shape[0]
    padded = jnp.pad(gate_rows.astype(jnp.float32), ((width - 1, 0), (0, 0)))
    mixed_pre = jnp.zeros((length, gate_rows.shape[1]), jnp.float32)
    for j in range(width):
        mixed_pre = mixed_pre + padded[j : j + length] * taps[j]
    return (mixed_pre, padded)


def gelu_slope(mixed_pre):
    return (
        0.5 * (1.0 + lax.erf(mixed_pre * root_half))
        + mixed_pre * jnp.exp(-0.5 * mixed_pre * mixed_pre) * density_norm
    )


def back_mix(slope_rows, taps, padded):
    width = taps.shape[0]
    length = slope_rows.shape[0]
    grown = jnp.pad(slope_rows, ((0, width - 1), (0, 0)))
    d_gate = jnp.zeros(slope_rows.shape, jnp.float32)
    for j in range(width):
        d_gate = d_gate + grown[width - 1 - j : width - 1 - j + length] * taps[j]
    tap_terms = jnp.stack(
        [jnp.sum(slope_rows * padded[j : j + length], axis=0) for j in range(width)]
    )
    return (d_gate, tap_terms)


def shards(x_late, x_early, w_gate, w_value, conv_taps, grad_hidden, sum_gate, sum_value, sum_taps):
    columns = w_gate.shape[1]
    factor = 1.0 / math.sqrt(x_late.shape[0] * lax.axis_size("fs") * lax.axis_size("tp"))
    gate_full, value_full = (
        lax.all_gather(w_gate, "fs", axis=0, tiled=True),
        lax.all_gather(w_value, "fs", axis=0, tiled=True),
    )
    block_rows = lax.all_gather(x_late, "tp", axis=0, tiled=True)
    gate_part = jnp.dot(block_rows, gate_full, preferred_element_type=jnp.float32).astype(
        jnp.bfloat16
    )
    value_part = jnp.dot(block_rows, value_full, preferred_element_type=jnp.float32).astype(
        jnp.bfloat16
    )
    projected = jnp.concatenate([gate_part, value_part], axis=1)
    gate_rows = projected[:, :columns]
    value_rows = projected[:, columns:]
    mixed_pre, padded = causal_mix(gate_rows, conv_taps)
    hidden = (jax.nn.gelu(mixed_pre, approximate=False) * value_rows.astype(jnp.float32)).astype(
        jnp.bfloat16
    )
    gathered = lax.all_gather(x_early, "tp", axis=0, tiled=True)
    gate_rows = jnp.dot(gathered, gate_full, preferred_element_type=jnp.float32).astype(
        jnp.bfloat16
    )
    value_rows = jnp.dot(gathered, value_full, preferred_element_type=jnp.float32).astype(
        jnp.bfloat16
    )
    mixed_pre, padded = causal_mix(gate_rows, conv_taps)
    upstream = grad_hidden.astype(jnp.float32)
    slope_rows = upstream * value_rows.astype(jnp.float32) * gelu_slope(mixed_pre)
    d_gate_f, tap_terms = back_mix(slope_rows, conv_taps, padded)
    d_gate = d_gate_f.astype(jnp.bfloat16)
    d_value = (upstream * jax.nn.gelu(mixed_pre, approximate=False)).astype(jnp.bfloat16)
    contract = (((1,), (1,)), ((), ()))
    grad_early = lax.psum_scatter(
        (
            lax.dot_general(d_gate, gate_full, contract, preferred_element_type=jnp.float32)
            + lax.dot_general(d_value, value_full, contract, preferred_element_type=jnp.float32)
        ).astype(jnp.bfloat16),
        "tp",
        scatter_dimension=0,
        tiled=True,
    )
    both_grads = jnp.concatenate([d_gate, d_value], axis=1)
    product = lax.dot_general(
        gathered, both_grads, (((0,), (0,)), ((), ())), preferred_element_type=jnp.float32
    )
    totals = lax.psum_scatter(
        (factor * product).astype(jnp.bfloat16), "fs", scatter_dimension=0, tiled=True
    ).astype(jnp.float32)
    gate_total = totals[:, :columns]
    value_total = totals[:, columns:]
    tap_total = lax.psum(factor * tap_terms, "fs")
    return (
        hidden,
        grad_early,
        sum_gate + gate_total,
        sum_value + value_total,
        sum_taps + tap_total,
    )


def solution(mesh):
    placed = (
        P(("fs", "tp"), None),
        P(("fs", "tp"), None),
        P("fs", "tp"),
        P("fs", "tp"),
        P(None, "tp"),
        P("fs", "tp"),
        P("fs", "tp"),
        P("fs", "tp"),
        P(None, "tp"),
    )
    return jax.shard_map(
        shards,
        mesh=mesh,
        in_specs=placed,
        out_specs=(
            P("fs", "tp"),
            P(("fs", "tp"), None),
            P("fs", "tp"),
            P("fs", "tp"),
            P(None, "tp"),
        ),
        check_vma=False,
    )
```

profile of v0, /device:TPU:0, one launch (start us, length us, event | category | flops | bytes accessed | tf_op | source)
XLA Modules:
  0.0 500.2 jit_solution(172343307863899647)
XLA Ops:
  7.2 0.7 all-gather.11.cloned.1.call-update
  7.9 0.0 all-gather.7.cloned.1.call-start
  7.9 0.7 all-gather.7.cloned.1.call-update
  8.7 0.7 all-gather.9.cloned.1.call-update
  9.4 0.5 all-gather.5.cloned.1.call-update
  10.0 0.0 reduce-scatter.5.cloned.1.call-start
  10.0 0.9 slice_reduce_fusion.2
  10.9 29.9 %all-gather.11.cloned.1.call-done = bf16[768,2048]{1,0:T(8,128)(2,1)} async-done(((bf16[192,2048]{1,0:T(8,128)(2,1)}), bf16[768,2048]{1,0:T(8,128)(2,1)}) %all-gather.11.cloned.1.call-update) | async-done | bytes 3145744 | tf_op jit(solution)/shard_map/all_gather | solution.py:62
  40.8 94.5 %all-gather.7.cloned.1.call-done = bf16[2048,1408]{1,0:T(8,128)(2,1)} async-done(((bf16[256,1408]{1,0:T(8,128)(2,1)}), bf16[2048,1408]{1,0:T(8,128)(2,1)}) %all-gather.7.cloned.1.call-update) | async-done | bytes 5767184 | tf_op jit(solution)/shard_map/all_gather | solution.py:45
  135.3 8.4 %fusion.30 = f32[768,1408]{1,0:T(8,128)S(1)} fusion(bf16[768,2048]{1,0:T(8,128)(2,1)} %all-gather.11.cloned.1.call-done, bf16[2048,1408]{1,0:T(8,128)(2,1)} %all-gather.7.cloned.1.call-done), kind=kOutput, calls=%fused_computation.62 | convolution fusion | flops 4431347712 | bytes 13238272 | tf_op jit(solution)/shard_map/dot_general | solution.py:63
  143.8 2.0 copy-done
  145.7 11.8 %fusion.2 = (bf16[768,1408]{1,0:T(8,128)(2,1)}, f32[768,1408]{1,0:T(8,128)}) fusion(bf16[768,1408]{1,0:T(8,128)(2,1)S(1)} %copy-done.2, f32[768,1408]{1,0:T(8,128)S(1)} %fusion.30, f32[1408]{0:T(1024)S(1)} %get-tuple-element.14, f32[1408]{0:T(1024)S(1)} %get-tuple-element.15, f32[1408]{0:T(1024)S(1)} %get-tuple-element.13), kind=kLoop, calls=%fused_computation.9 | loop fusion | flops 77856768 | bytes 12993024 | tf_op jit(solution)/shard_map/convert_element_type | solution.py:74
  157.6 70.5 %all-gather.9.cloned.1.call-done = bf16[2048,1408]{1,0:T(8,128)(2,1)} async-done(((bf16[256,1408]{1,0:T(8,128)(2,1)}), bf16[2048,1408]{1,0:T(8,128)(2,1)}) %all-gather.9.cloned.1.call-update) | async-done | bytes 5767184 | tf_op jit(solution)/shard_map/all_gather | solution.py:46
  228.0 9.8 %fusion.1 = f32[768,1408]{1,0:T(8,128)S(1)} fusion(bf16[768,1408]{1,0:T(8,128)(2,1)S(1)} %copy-done.2, f32[768,1408]{1,0:T(8,128)} %get-tuple-element.17, bf16[768,2048]{1,0:T(8,128)(2,1)} %all-gather.11.cloned.1.call-done, bf16[2048,1408]{1,0:T(8,128)(2,1)} %all-gather.9.cloned.1.call-done), kind=kOutput, calls=%fused_computation.8 | convolution fusion | flops 4443242496 | bytes 19726336 | tf_op jit(solution)/shard_map/dot_general | solution.py:66
  237.9 3.0 multiply_reduce_fusion.2
  240.9 1.3 copy-done.4
  242.3 12.1 %fusion = bf16[2048,2816]{0,1:T(8,128)(2,1)} fusion(bf16[768,2048]{1,0:T(8,128)(2,1)S(1)} %copy-done.7, bf16[768,1408]{1,0:T(8,128)(2,1)S(1)} %copy-done.3, bf16[768,1408]{1,0:T(8,128)(2,1)S(1)} %get-tuple-element.18), kind=kOutput, calls=%fused_computation.1 | convolution fusion | flops 8878555136 | bytes 19005440 | tf_op jit(solution)/shard_map/dot_general | solution.py:86
  254.4 0.0 reduce-scatter.3.cloned.1.call-start
  254.5 7.8 %fusion.33 = f32[768,2048]{1,0:T(8,128)S(1)} fusion(bf16[768,1408]{1,0:T(8,128)(2,1)} %copy-done.4, bf16[2048,1408]{1,0:T(8,128)(2,1)} %all-gather.7.cloned.1.call-done), kind=kOutput, calls=%fused_computation.74 | convolution fusion | flops 4429185024 | bytes 14221312 | tf_op jit(solution)/shard_map/dot_general | solution.py:78
  262.3 9.2 %add_convert_fusion = bf16[768,2048]{1,0:T(8,128)(2,1)} fusion(f32[768,2048]{1,0:T(8,128)S(1)} %fusion.33, bf16[768,1408]{1,0:T(8,128)(2,1)S(1)} %copy-done.3, bf16[2048,1408]{1,0:T(8,128)(2,1)} %all-gather.9.cloned.1.call-done), kind=kOutput, calls=%fused_computation.5 | convolution fusion | flops 4432330752 | bytes 17367040 | tf_op jit(solution)/shard_map/dot_general | solution.py:79
  271.5 1.8 copy.14
  273.3 1.8 copy.15
  275.2 36.6 %psum.7 = f32[3,1408]{1,0:T(4,128)S(1)} all-reduce(f32[3,1408]{1,0:T(4,128)S(1)} %maximum_multiply_fusion), channel_id=1, replica_groups=mesh['fs'=8,'tp'=4] {'fs'}, use_global_device_ids=true, to_apply=%region_5.6 | all-reduce | flops 4224 | bytes 33792 | tf_op jit(solution)/shard_map/psum | solution.py:94
  311.8 0.6 add.59
  312.4 9.0 %fusion.31 = f32[768,1408]{1,0:T(8,128)S(1)} fusion(bf16[768,2048]{1,0:T(8,128)(2,1)} %all-gather.5.cloned.1.call-done, bf16[2048,1408]{1,0:T(8,128)(2,1)} %all-gather.7.cloned.1.call-done), kind=kOutput, calls=%fused_computation.66 | convolution fusion | flops 4431347712 | bytes 13238272 | tf_op jit(solution)/shard_map/dot_general | solution.py:49
  321.4 19.9 %fusion.6 = bf16[768,1408]{1,0:T(8,128)(2,1)} fusion(f32[768,1408]{1,0:T(8,128)S(1)} %fusion.31, bf16[768,2048]{1,0:T(8,128)(2,1)S(1)} %copy-done.6, bf16[2048,1408]{1,0:T(8,128)(2,1)} %all-gather.9.cloned.1.call-done, f32[1408]{0:T(1024)S(1)} %get-tuple-element.14, f32[1408]{0:T(1024)S(1)} %get-tuple-element.15, f32[1408]{0:T(1024)S(1)} %get-tuple-element.13), kind=kOutput, calls=%fused_computation.13 | convolution fusion | flops 4508123136 | bytes 15417856 | tf_op jit(solution)/shard_map/dot_general | solution.py:52
  341.3 112.0 %reduce-scatter.5.cloned.1.call-done = bf16[256,2816]{0,1:T(8,128)(2,1)} async-done(((bf16[2048,2816]{0,1:T(8,128)(2,1)}), bf16[256,2816]{0,1:T(8,128)(2,1)}) %reduce-scatter.5.cloned.1.call-update) | async-done | bytes 1441808 | tf_op jit(solution)/shard_map/reduce_scatter | solution.py:89
  453.4 1.6 convert_element_type.68
  454.9 1.9 slice_add_fusion
  456.9 2.9 copy.16
  459.8 3.2 copy.17
  463.0 30.4 %reduce-scatter.3.cloned.1.call-done = bf16[192,2048]{1,0:T(8,128)(2,1)} async-done(((bf16[768,2048]{1,0:T(8,128)(2,1)}), bf16[192,2048]{1,0:T(8,128)(2,1)}) %reduce-scatter.3.cloned.1.call-update) | async-done | bytes 786448 | tf_op jit(solution)/shard_map/reduce_scatter | solution.py:76
  (24 shorter events, 0.2 us)
Async XLA Ops:
  7.2 33.6 %all-gather.11.cloned.1.call-start = ((), (), s32[]{:S(2)}) async-start(), calls=%async_computation.5 | async-start | bytes 3932160 | tf_op jit(solution)/shard_map/all_gather | solution.py:62
  7.9 127.4 %all-gather.7.cloned.1.call-start = ((), (), s32[]{:S(2)}) async-start(), calls=%async_computation.3 | async-start | bytes 6488064 | tf_op jit(solution)/shard_map/all_gather | solution.py:45
  8.6 219.4 %all-gather.9.cloned.1.call-start = ((), (), s32[]{:S(2)}) async-start(), calls=%async_computation.4 | async-start | bytes 6488064 | tf_op jit(solution)/shard_map/all_gather | solution.py:46
  9.4 303.0 %all-gather.5.cloned.1.call-start = ((), (), s32[]{:S(2)}) async-start(), calls=%async_computation.2 | async-start | bytes 3932160 | tf_op jit(solution)/shard_map/all_gather | solution.py:48
  10.0 443.4 %reduce-scatter.5.cloned.1.call-start = ((), (), s32[]{:S(2)}) async-start(), calls=%async_computation.7 | async-start | bytes 12976128 | tf_op jit(solution)/shard_map/reduce_scatter | solution.py:89
  10.9 134.8 %copy-start.2 = (bf16[768,1408]{1,0:T(8,128)(2,1)S(1)}, bf16[768,1408]{1,0:T(8,128)(2,1)}, u32[]{:S(2)}) copy-start(bf16[768,1408]{1,0:T(8,128)(2,1)} %param.14) | copy-start | bytes 6488068
  143.7 2.0 copy-start
  228.0 9.9 %copy-start.1 = (f32[768,1408]{1,0:T(8,128)S(1)}, f32[768,1408]{1,0:T(8,128)}, u32[]{:S(2)}) copy-start(f32[768,1408]{1,0:T(8,128)} %copy-done) | copy-start | bytes 12976132
  237.9 4.4 copy-start.3
  237.9 4.4 copy-start.7
  240.9 1.3 copy-start.4
  254.4 238.9 %reduce-scatter.3.cloned.1.call-start = ((), (), s32[]{:S(2)}) async-start(), calls=%async_computation.6 | async-start | bytes 3932160 | tf_op jit(solution)/shard_map/reduce_scatter | solution.py:76
  271.5 40.3 %copy-start.5 = (f32[3,1408]{1,0:T(4,128)S(1)}, f32[3,1408]{1,0:T(4,128)}, u32[]{:S(2)}) copy-start(f32[3,1408]{1,0:T(4,128)} %param.17) | copy-start | bytes 50692
  312.4 9.0 %copy-start.6 = (bf16[768,2048]{1,0:T(8,128)(2,1)S(1)}, bf16[768,2048]{1,0:T(8,128)(2,1)}, u32[]{:S(2)}) copy-start(bf16[768,2048]{1,0:T(8,128)(2,1)} %all-gather.5.cloned.1.call-done) | copy-start | bytes 9437188
Sparse Core Ops, SparseCore 0:
  9.5 31.2 all-gather.10
  43.0 92.3 all-gather.6
  137.5 90.4 all-gather.8
  229.4 26.6 all-gather.4
  259.6 193.6 reduce-scatter.4
  456.3 37.0 reduce-scatter.2
where the time goes:
time: 501 us; the launch traced here: 500 us
  waiting for transfers between devices  340 us (68%)
  matrix products  76.3 us (15%)
  blocking collectives  36.6 us (7%)
  other arithmetic  19 us (4%)
  between operations  14.3 us (3%)
  local copies, waits for them, and re-layouts  14 us (3%)
    reduce_scatter x1, waiting for transfers between devices, shards(): lax.psum_scatter((factor * product).astype(jnp.bfloat16), 'fs', scatter_d...  112 us
    all_gather x1, waiting for transfers between devices, shards(): lax.all_gather(w_gate, 'fs', axis=0, tiled=True)  94.5 us
    all_gather x1, waiting for transfers between devices, shards(): lax.all_gather(w_value, 'fs', axis=0, tiled=True)  70.5 us
    psum x1, blocking collectives, shards(): tap_total = lax.psum(factor * tap_terms, 'fs')  36.6 us
    reduce_scatter x1, waiting for transfers between devices, shards(): lax.psum_scatter((lax.dot_general(d_gate, gate_full, contract, preferred_...  30.4 us
    all_gather x1, waiting for transfers between devices, shards(): gathered = lax.all_gather(x_early, 'tp', axis=0, tiled=True)  29.9 us
    dot_general x1, matrix products, shards(): jnp.dot(block_rows, value_full, preferred_element_type=jnp.float32)  19.9 us
    unnamed x20, local copies, waits for them, and re-layouts  13.1 us
  transfers between devices with their start and end apart: 6, of which 5 were waited for; matrix products, arithmetic and copies ran while one was open for 21% of the time, Pallas kernels for 0%

commit v1 on v0

--- a/solution.py
+++ b/solution.py
@@ -59,7 +59,12 @@
     hidden = (jax.nn.gelu(mixed_pre, approximate=False) * value_rows.astype(jnp.float32)).astype(
         jnp.bfloat16
     )
-    gathered = lax.all_gather(x_early, "tp", axis=0, tiled=True)
+    ring = [x_early]
+    for hop in range(3):
+        ring.append(lax.ppermute(ring[-1], "tp", [(dev, (dev + 1) % 4) for dev in range(4)]))
+    gathered = jnp.roll(
+        jnp.concatenate(ring[::-1], axis=0), (lax.axis_index("tp") + 1) * ring[0].shape[0], axis=0
+    )
     gate_rows = jnp.dot(gathered, gate_full, preferred_element_type=jnp.float32).astype(
         jnp.bfloat16
     )

time: 501 us -> 470 us (0.938)
  waiting for transfers between devices: 340 us -> 308 us
    all_gather x1, waiting for transfers between devices: 94.5 us -> 53.8 us  [shards(): lax.all_gather(w_gate, 'fs', axis=0, tiled=True)]
    ppermute x0 -> x3, waiting for transfers between devices: none -> 33.6 us  [shards(): lax.ppermute(ring[-1], 'tp', [(dev, (dev + 1) % 4) for dev in range(4)])]
    all_gather x1 -> x0, waiting for transfers between devices: 29.9 us -> none  [shards(): gathered = lax.all_gather(x_early, 'tp', axis=0, tiled=True)]
    reduce_scatter x1, waiting for transfers between devices: 30.4 us -> 36.3 us  [shards(): lax.psum_scatter((lax.dot_general(d_gate, gate_full, contract, preferred_...]
    unnamed x20 -> x27, local copies, waits for them, and re-layouts: 13.1 us -> 10.1 us
  transfers between devices with their start and end apart: 6 -> 8, of which waited for: 5 -> 7; matrix products, arithmetic and copies ran while one was open for 21% -> 23% of each run, Pallas kernels for 0% -> 0%
where the time goes in v1:
time: 470 us; the launch traced here: 469 us
  waiting for transfers between devices  308 us (66%)
  matrix products  80.4 us (17%)
  blocking collectives  35.6 us (8%)
  other arithmetic  19 us (4%)
  between operations  14 us (3%)
  local copies, waits for them, and re-layouts  11.9 us (3%)
    reduce_scatter x1, waiting for transfers between devices, shards(): lax.psum_scatter((factor * product).astype(jnp.bfloat16), 'fs', scatter_d...  112 us
    all_gather x1, waiting for transfers between devices, shards(): lax.all_gather(w_value, 'fs', axis=0, tiled=True)  70.4 us
    all_gather x1, waiting for transfers between devices, shards(): lax.all_gather(w_gate, 'fs', axis=0, tiled=True)  53.8 us
    reduce_scatter x1, waiting for transfers between devices, shards(): lax.psum_scatter((lax.dot_general(d_gate, gate_full, contract, preferred_...  36.3 us
    psum x1, blocking collectives, shards(): tap_total = lax.psum(factor * tap_terms, 'fs')  35.6 us
    ppermute x3, waiting for transfers between devices, shards(): lax.ppermute(ring[-1], 'tp', [(dev, (dev + 1) % 4) for dev in range(4)])  33.6 us
    dot_general x1, matrix products, shards(): jnp.dot(block_rows, value_full, preferred_element_type=jnp.float32)  19.9 us
    dot_general x1, matrix products, shards(): lax.dot_general(gathered, both_grads, (((0,), (0,)), ((), ())), preferred...  15.1 us
  transfers between devices with their start and end apart: 8, of which 7 were waited for; matrix products, arithmetic and copies ran while one was open for 23% of the time, Pallas kernels for 0%

profile of v1, /device:TPU:0, one launch (start us, length us, event | category | flops | bytes accessed | tf_op | source)
XLA Modules:
  0.0 469.3 jit_solution(16289531635578527128)
XLA Ops:
  7.2 0.7 all-gather.6.cloned.1.call-update
  8.0 0.7 all-gather.8.cloned.1.call-update
  9.2 11.8 %collective-permute-done = bf16[192,2048]{1,0:T(8,128)(2,1)S(1)} collective-permute-done((bf16[192,2048]{1,0:T(8,128)(2,1)}, bf16[192,2048]{1,0:T(8,128)(2,1)S(1)}, u32[]{:S(2)}, u32[]{:S(2)}) %collective-permute-start) | collective-permute-done | bytes 786464 | tf_op jit(solution)/shard_map/ppermute | solution.py:64
  21.1 11.4 %collective-permute-done.1 = bf16[192,2048]{1,0:T(8,128)(2,1)S(1)} collective-permute-done((bf16[192,2048]{1,0:T(8,128)(2,1)S(1)}, bf16[192,2048]{1,0:T(8,128)(2,1)S(1)}, u32[]{:S(2)}, u32[]{:S(2)}) %collective-permute-start.1) | collective-permute-done | bytes 786464 | tf_op jit(solution)/shard_map/ppermute | solution.py:64
  32.6 0.9 slice_reduce_fusion.2
  33.5 10.4 %collective-permute-done.2 = bf16[192,2048]{1,0:T(8,128)(2,1)S(1)} collective-permute-done((bf16[192,2048]{1,0:T(8,128)(2,1)S(1)}, bf16[192,2048]{1,0:T(8,128)(2,1)S(1)}, u32[]{:S(2)}, u32[]{:S(2)}) %collective-permute-start.2) | collective-permute-done | bytes 786464 | tf_op jit(solution)/shard_map/ppermute | solution.py:64
  43.9 0.9 constant_dynamic-update-slice_fusion.7
  44.8 1.0 constant_dynamic-update-slice_fusion.6
  45.8 1.0 constant_dynamic-update-slice_fusion.5
  46.7 1.0 constant_dynamic-update-slice_fusion.4
  47.7 0.9 constant_dynamic-update-slice_fusion.3
  48.7 0.9 constant_dynamic-update-slice_fusion.2
  49.6 0.9 constant_dynamic-update-slice_fusion.1
  50.5 1.0 constant_dynamic-update-slice_fusion
  51.5 53.8 %all-gather.6.cloned.1.call-done = bf16[2048,1408]{1,0:T(8,128)(2,1)} async-done(((bf16[256,1408]{1,0:T(8,128)(2,1)}), bf16[2048,1408]{1,0:T(8,128)(2,1)}) %all-gather.6.cloned.1.call-update) | async-done | bytes 5767184 | tf_op jit(solution)/shard_map/all_gather | solution.py:45
  105.2 8.4 %fusion.29 = f32[768,1408]{1,0:T(8,128)S(1)} fusion(bf16[2048,1408]{1,0:T(8,128)(2,1)} %all-gather.6.cloned.1.call-done, bf16[1536,2048]{1,0:T(8,128)(2,1)} %constant_dynamic-update-slice_fusion, s32[]{:T(128)S(6)} %select_n.14), kind=kOutput, calls=%fused_computation.61 | convolution fusion | flops 4431347712 | bytes 13238276 | tf_op jit(solution)/shard_map/dot_general | solution.py:68
  113.7 2.0 copy-done
  115.7 11.8 %fusion.1 = (bf16[768,1408]{1,0:T(8,128)(2,1)}, f32[768,1408]{1,0:T(8,128)}) fusion(bf16[768,1408]{1,0:T(8,128)(2,1)S(1)} %copy-done.3, f32[768,1408]{1,0:T(8,128)S(1)} %fusion.29, f32[1408]{0:T(1024)S(1)} %get-tuple-element.9, f32[1408]{0:T(1024)S(1)} %get-tuple-element.10, f32[1408]{0:T(1024)S(1)} %get-tuple-element.8), kind=kLoop, calls=%fused_computation.8 | loop fusion | flops 77856768 | bytes 12993024 | tf_op jit(solution)/shard_map/convert_element_type | solution.py:79
  127.5 70.4 %all-gather.8.cloned.1.call-done = bf16[2048,1408]{1,0:T(8,128)(2,1)} async-done(((bf16[256,1408]{1,0:T(8,128)(2,1)}), bf16[2048,1408]{1,0:T(8,128)(2,1)}) %all-gather.8.cloned.1.call-update) | async-done | bytes 5767184 | tf_op jit(solution)/shard_map/all_gather | solution.py:46
  197.9 9.9 %fusion = f32[768,1408]{1,0:T(8,128)S(1)} fusion(bf16[768,1408]{1,0:T(8,128)(2,1)S(1)} %copy-done.3, f32[768,1408]{1,0:T(8,128)} %get-tuple-element.12, bf16[2048,1408]{1,0:T(8,128)(2,1)} %all-gather.8.cloned.1.call-done, bf16[1536,2048]{1,0:T(8,128)(2,1)} %constant_dynamic-update-slice_fusion, s32[]{:T(128)S(6)} %select_n.14), kind=kOutput, calls=%fused_computation.7 | convolution fusion | flops 4443242496 | bytes 19726340 | tf_op jit(solution)/shard_map/dot_general | solution.py:71
  207.9 3.0 multiply_reduce_fusion.2
  210.9 1.3 copy-done.5
  212.2 15.1 %multiply_convert_fusion = bf16[2048,2816]{1,0:T(8,128)(2,1)} fusion(bf16[768,1408]{1,0:T(8,128)(2,1)S(1)} %copy-done.4, bf16[768,1408]{1,0:T(8,128)(2,1)S(1)} %get-tuple-element.13, bf16[1536,2048]{1,0:T(8,128)(2,1)} %constant_dynamic-update-slice_fusion, s32[]{:T(128)S(6)} %select_n.14), kind=kOutput, calls=%fused_computation | convolution fusion | flops 8878555136 | bytes 19005444 | tf_op jit(solution)/shard_map/dot_general | solution.py:91
  227.4 7.8 %fusion.38 = f32[768,2048]{1,0:T(8,128)S(1)} fusion(bf16[768,1408]{1,0:T(8,128)(2,1)} %copy-done.5, bf16[2048,1408]{1,0:T(8,128)(2,1)} %all-gather.6.cloned.1.call-done), kind=kOutput, calls=%fused_computation.87 | convolution fusion | flops 4429185024 | bytes 14221312 | tf_op jit(solution)/shard_map/dot_general | solution.py:83
  235.2 10.2 %add_convert_fusion = bf16[768,2048]{1,0:T(8,128)(2,1)} fusion(f32[768,2048]{1,0:T(8,128)S(1)} %fusion.38, bf16[768,1408]{1,0:T(8,128)(2,1)S(1)} %copy-done.4, bf16[2048,1408]{1,0:T(8,128)(2,1)} %all-gather.8.cloned.1.call-done), kind=kOutput, calls=%fused_computation.4 | convolution fusion | flops 4432330752 | bytes 17367040 | tf_op jit(solution)/shard_map/dot_general | solution.py:84
  245.5 35.6 %psum.7 = f32[3,1408]{1,0:T(4,128)S(1)} all-reduce(f32[3,1408]{1,0:T(4,128)S(1)} %maximum_multiply_fusion), channel_id=1, replica_groups=mesh['fs'=8,'tp'=4] {'fs'}, use_global_device_ids=true, to_apply=%region_5.6 | all-reduce | flops 4224 | bytes 33792 | tf_op jit(solution)/shard_map/psum | solution.py:99
  281.8 9.0 %fusion.30 = f32[768,1408]{1,0:T(8,128)S(1)} fusion(bf16[768,2048]{1,0:T(8,128)(2,1)} %all-gather.4.cloned.1.call-done, bf16[2048,1408]{1,0:T(8,128)(2,1)} %all-gather.6.cloned.1.call-done), kind=kOutput, calls=%fused_computation.65 | convolution fusion | flops 4431347712 | bytes 13238272 | tf_op jit(solution)/shard_map/dot_general | solution.py:49
  290.8 19.9 %fusion.5 = bf16[768,1408]{1,0:T(8,128)(2,1)} fusion(f32[768,1408]{1,0:T(8,128)S(1)} %fusion.30, bf16[768,2048]{1,0:T(8,128)(2,1)S(1)} %copy-done.9, bf16[2048,1408]{1,0:T(8,128)(2,1)} %all-gather.8.cloned.1.call-done, f32[1408]{0:T(1024)S(1)} %get-tuple-element.9, f32[1408]{0:T(1024)S(1)} %get-tuple-element.10, f32[1408]{0:T(1024)S(1)} %get-tuple-element.8), kind=kOutput, calls=%fused_computation.12 | convolution fusion | flops 4508123136 | bytes 15417856 | tf_op jit(solution)/shard_map/dot_general | solution.py:52
  310.8 112.0 %reduce-scatter.5.cloned.1.call-done = bf16[256,2816]{1,0:T(8,128)(2,1)} async-done(((bf16[2048,2816]{1,0:T(8,128)(2,1)}), bf16[256,2816]{1,0:T(8,128)(2,1)}) %reduce-scatter.5.cloned.1.call-update) | async-done | bytes 1441808 | tf_op jit(solution)/shard_map/reduce_scatter | solution.py:94
  422.7 1.7 convert_element_type.64
  424.5 1.9 slice_add_fusion
  426.4 36.3 %reduce-scatter.3.cloned.1.call-done = bf16[192,2048]{1,0:T(8,128)(2,1)} async-done(((bf16[768,2048]{1,0:T(8,128)(2,1)}), bf16[192,2048]{1,0:T(8,128)(2,1)}) %reduce-scatter.3.cloned.1.call-update) | async-done | bytes 786448 | tf_op jit(solution)/shard_map/reduce_scatter | solution.py:81
  (35 shorter events, 1.6 us)
Async XLA Ops:
  7.2 39.6 %copy-start.2 = (bf16[192,2048]{1,0:T(8,128)(2,1)S(1)}, bf16[192,2048]{1,0:T(8,128)(2,1)}, u32[]{:S(2)}) copy-start(bf16[192,2048]{1,0:T(8,128)(2,1)} %param.10) | copy-start | bytes 2359300
  7.2 98.1 %all-gather.6.cloned.1.call-start = ((), (), s32[]{:S(2)}) async-start(), calls=%async_computation.3 | async-start | bytes 6488064 | tf_op jit(solution)/shard_map/all_gather | solution.py:45
  7.9 190.0 %all-gather.8.cloned.1.call-start = ((), (), s32[]{:S(2)}) async-start(), calls=%async_computation.4 | async-start | bytes 6488064 | tf_op jit(solution)/shard_map/all_gather | solution.py:46
  8.7 273.1 %all-gather.4.cloned.1.call-start = ((), (), s32[]{:S(2)}) async-start(), calls=%async_computation.2 | async-start | bytes 3932160 | tf_op jit(solution)/shard_map/all_gather | solution.py:48
  8.7 12.3 %collective-permute-start = (bf16[192,2048]{1,0:T(8,128)(2,1)}, bf16[192,2048]{1,0:T(8,128)(2,1)S(1)}, u32[]{:S(2)}, u32[]{:S(2)}) collective-permute-start(bf16[192,2048]{1,0:T(8,128)(2,1)} %param.10), channel_id=1, source_target_pairs={{0,1},{1,2},{2,3},{3,0},{4,5},{5,6},{6,7},{7,4},{8,9},{9,10},{10,1... | collective-permute-start | bytes 2359304 | tf_op jit(solution)/shard_map/ppermute | solution.py:64
  21.0 11.4 %collective-permute-start.1 = (bf16[192,2048]{1,0:T(8,128)(2,1)S(1)}, bf16[192,2048]{1,0:T(8,128)(2,1)S(1)}, u32[]{:S(2)}, u32[]{:S(2)}) collective-permute-start(bf16[192,2048]{1,0:T(8,128)(2,1)S(1)} %collective-permute-done), channel_id=1, source_target_pairs={{0,1},{1,2},{2,3},{3,0},{4,5},{5,6},{6,7},{7,4},{8,9},{9,10},{10,1... | collective-permute-start | bytes 2359304 | tf_op jit(solution)/shard_map/ppermute | solution.py:64
  32.5 11.4 %collective-permute-start.2 = (bf16[192,2048]{1,0:T(8,128)(2,1)S(1)}, bf16[192,2048]{1,0:T(8,128)(2,1)S(1)}, u32[]{:S(2)}, u32[]{:S(2)}) collective-permute-start(bf16[192,2048]{1,0:T(8,128)(2,1)S(1)} %collective-permute-done.1), channel_id=1, source_target_pairs={{0,1},{1,2},{2,3},{3,0},{4,5},{5,6},{6,7},{7,4},{8,9},{9,10},{10,1... | collective-permute-start | bytes 2359304 | tf_op jit(solution)/shard_map/ppermute | solution.py:64
  32.5 390.3 %reduce-scatter.5.cloned.1.call-start = ((), (), s32[]{:S(2)}) async-start(), calls=%async_computation.6 | async-start | bytes 12976128 | tf_op jit(solution)/shard_map/reduce_scatter | solution.py:94
  51.5 64.2 %copy-start.3 = (bf16[768,1408]{1,0:T(8,128)(2,1)S(1)}, bf16[768,1408]{1,0:T(8,128)(2,1)}, u32[]{:S(2)}) copy-start(bf16[768,1408]{1,0:T(8,128)(2,1)} %param.14) | copy-start | bytes 6488068
  113.7 2.0 copy-start
  197.9 9.9 %copy-start.1 = (f32[768,1408]{1,0:T(8,128)S(1)}, f32[768,1408]{1,0:T(8,128)}, u32[]{:S(2)}) copy-start(f32[768,1408]{1,0:T(8,128)} %copy-done) | copy-start | bytes 12976132
  207.9 4.4 copy-start.4
  210.9 1.3 copy-start.5
  227.4 235.4 %reduce-scatter.3.cloned.1.call-start = ((), (), s32[]{:S(2)}) async-start(), calls=%async_computation.5 | async-start | bytes 3932160 | tf_op jit(solution)/shard_map/reduce_scatter | solution.py:81
  235.2 46.0 %copy-start.8 = (f32[3,1408]{1,0:T(4,128)S(1)}, f32[3,1408]{1,0:T(4,128)}, u32[]{:S(2)}) copy-start(f32[3,1408]{1,0:T(4,128)} %param.17) | copy-start | bytes 50692
  281.8 9.0 %copy-start.9 = (bf16[768,2048]{1,0:T(8,128)(2,1)S(1)}, bf16[768,2048]{1,0:T(8,128)(2,1)}, u32[]{:S(2)}) copy-start(bf16[768,2048]{1,0:T(8,128)(2,1)} %all-gather.4.cloned.1.call-done) | copy-start | bytes 9437188
  310.8 113.6 %copy-start.6 = (f32[256,1408]{1,0:T(8,128)S(1)}, f32[256,1408]{1,0:T(8,128)}, u32[]{:S(2)}) copy-start(f32[256,1408]{1,0:T(8,128)} %param.16) | copy-start | bytes 4325380
  422.7 1.8 copy-start.7
Sparse Core Ops, SparseCore 0:
  10.2 95.0 all-gather.5
  107.4 90.4 all-gather.7
  199.5 26.6 all-gather.3
  229.7 193.0 reduce-scatter.4
  425.7 36.9 reduce-scatter.2
